TPU v7x, 512 devices: a 8x2x16 block of a 8x8x16 slice. The times are simulated.
512 devices in a mesh: grp: 2 (over y), dp: 8 (over x), kv: 16 (over z), tp: 2 (over core).
Axes of the slice: x: 8, y: 2, z: 16, core: 2. Of those that a mesh axis runs over, the one named last changes fastest.
The devices are a block of a 8x8x16 slice.
Arguments:
- inputs: bfloat16 [512, 4096], P(('grp', 'dp'), 'kv'), parts along dimension 0, may hold values from -6 to 6
- gain_in: float32 [4096], P('kv'), may hold values from 0.1 to 1.9
- w_gate: bfloat16 [4096, 2048], P('kv', 'tp'), may hold values from -0.09375 to 0.09375
- w_input: bfloat16 [4096, 2048], P('kv', 'tp'), may hold values from -0.09375 to 0.09375
- w_bproj: bfloat16 [4096, 1024], P('kv', 'tp'), may hold values from -0.09375 to 0.09375
- w_cproj: bfloat16 [4096, 1024], P('kv', 'tp'), may hold values from -0.09375 to 0.09375
- w_step: bfloat16 [4096, 32], P('kv', 'tp'), may hold values from -0.09375 to 0.09375
- conv_input: float32 [4, 2048], P(None, 'tp'), may hold values from -3 to 3
- conv_bproj: float32 [4, 1024], P(None, 'tp'), may hold values from -3 to 3
- conv_cproj: float32 [4, 1024], P(None, 'tp'), may hold values from -3 to 3
- tail_input: bfloat16 [512, 3, 2048], P(('grp', 'dp', 'kv'), None, 'tp'), parts along dimension 0, may hold values from -6 to 6
- tail_bproj: bfloat16 [512, 3, 1024], P(('grp', 'dp', 'kv'), None, 'tp'), parts along dimension 0, may hold values from -6 to 6
- tail_cproj: bfloat16 [512, 3, 1024], P(('grp', 'dp', 'kv'), None, 'tp'), parts along dimension 0, may hold values from -6 to 6
- step_bias: float32 [32], P('tp'), may hold values from -3 to 0
- decay_log: float32 [32], P('tp'), may hold values from -2 to 2
- block_input: bfloat16 [512, 128, 2048], P(('grp', 'dp', 'kv'), None, 'tp'), parts along dimension 0, may hold values from -6 to 6
- block_bproj: bfloat16 [512, 128, 1024], P(('grp', 'dp', 'kv'), None, 'tp'), parts along dimension 0, may hold values from -0.59765625 to 0.59765625
- block_step: float32 [512, 128, 32], P(('grp', 'dp', 'kv'), None, 'tp'), parts along dimension 0, may hold values from 0.005 to 0.2
- lengths: int32 [512], P(('grp', 'dp', 'kv')), parts along dimension 0, may hold values from 1 to 127, 8192 in all
- state: float32 [512, 32, 64, 128], P(('grp', 'dp', 'kv'), 'tp'), parts along dimension 0, may hold values from -0.6 to 0.6
- gain_mix: float32 [2048], P('tp'), may hold values from 0.1 to 1.9
- w_out: bfloat16 [2048, 4096], P('tp', 'kv'), may hold values from -0.125 to 0.125
- gain_mlp: float32 [4096], P(('kv', 'tp')), may hold values from 0.1 to 1.9
- w_up: bfloat16 [4096, 16384], P(('kv', 'tp'), 'dp'), may hold values from -0.09375 to 0.09375
- w_down: bfloat16 [16384, 4096], P('dp', ('kv', 'tp')), may hold values from -0.046875 to 0.046875
Outputs:
- layer_out: bfloat16 [512, 4096], P(('grp', 'dp'), ('kv', 'tp')), parts along dimension 0
There are 2 independent parts, one for each index of `grp`. A program takes and returns all parts, laid end to end along the dimension named above; an argument that names none is the same for every part. Nothing has to cross between parts.
Inputs may be any that keep to these rules, and one draw needn't show every extreme that they name: `lengths`: the number of live positions before the new token in each sequence's current block; the largest equals 127 in every draw.
All inputs are finite; a program needn't handle non-finite values.
Results may differ from a plain program's by a relative error of at most 0.012.
Values may be sent and summed in bfloat16 or wider, within the bound.
No kernel may reach another device: no remote copies, remote signals or barrier semaphores. Data moves between devices by JAX's collectives and lax.ppermute only.
A program may use at most 64 MiB of HBM per device.

v0:
```python
import math
import jax
import jax.numpy as jnp
from jax import lax
from jax.sharding import PartitionSpec as P

D = 4096
HEAD_DIM = 64
D_STATE = 128
TAPS = 4
SSM_WIDTH = 2048
EPS = 1e-06


def in_blocks(shard, dim, size):
    before, after = (shard.shape[:dim], shard.shape[dim + 1 :])
    return jnp.moveaxis(shard.reshape(*before, size, -1, *after), dim, 0)


def sent_and_summed(shard, axis, dim):
    size = lax.axis_size(axis)
    tiles = lax.all_to_all(in_blocks(shard, dim, size), axis, 0, 0, tiled=True)
    return jnp.sum(tiles, axis=0)


def sent_together(arrays, axis, dim, along):
    widths = [math.prod(a.shape[along:]) for a in arrays]
    both = jnp.concatenate(
        [a.reshape(*a.shape[:along], w) for a, w in zip(arrays, widths)], axis=along
    )
    whole = sent_and_summed(both, axis, dim)
    tiles = jnp.split(whole, [sum(widths[:k]) for k in range(1, len(widths))], axis=along)
    return tuple((b.reshape(*whole.shape[:along], *a.shape[along:]) for a, b in zip(arrays, tiles)))


def gathered_total(shard, axis):
    return lax.all_gather(shard, axis).sum(0)


def from_everyone(shard, axis):
    size = lax.axis_size(axis)
    return lax.all_to_all(
        jnp.broadcast_to(shard[None], (size, *shard.shape)), axis, 0, 0, tiled=True
    )


def joined_along(tiles, dim):
    dims = list(tiles.shape[1:])
    dims[dim] *= tiles.shape[0]
    return jnp.moveaxis(tiles, 0, dim).reshape(dims)


def gather_directly(shard, axis, dim):
    tiles = from_everyone(shard, axis)
    return joined_along(tiles, dim)


def in_one_piece(arrays, axis, dim, along):
    ends, at = ([], 0)
    for a in arrays[:-1]:
        at += a.shape[along]
        ends.append(at)
    both = jnp.concatenate(arrays, axis=along)
    return tuple(jnp.split(lax.all_gather(both, axis, axis=dim, tiled=True), ends, axis=along))


def of_everyone(shard, axis):
    everything = from_everyone(shard, axis)
    return jnp.sum(everything, axis=0)


def summed_on_arrival(shard, axis, dim):
    tiles = in_blocks(shard, dim, lax.axis_size(axis))
    arrived = lax.all_to_all(tiles, axis, split_axis=0, concat_axis=0, tiled=True)
    return arrived.astype(jnp.float32).sum(axis=0)


def stacked_from(shard, axes, order):
    tiles = shard[None]
    for k in order:
        tiles = lax.all_gather(tiles, axes[k], axis=0, tiled=True)
    current = [lax.axis_size(axes[k]) for k in reversed(order)]
    tiles = tiles.reshape(*current, *shard.shape)
    turned = sorted(range(len(order)), key=lambda place: order[len(order) - 1 - place])
    return tiles.transpose(*turned, *range(len(order), tiles.ndim)).reshape(-1, *shard.shape)


def gathered_by_axis(shard, axes, order, dim):
    return joined_along(stacked_from(shard, axes, order), dim)


def convolve(history, weights, newest):
    summed = weights[TAPS - 1] * newest
    for offset in range(TAPS - 1):
        summed = summed + weights[offset] * history[:, offset].astype(jnp.float32)
    return jax.nn.silu(summed)


def per_device(
    inputs,
    gain_in,
    w_gate,
    w_input,
    w_bproj,
    w_cproj,
    w_step,
    conv_input,
    conv_bproj,
    conv_cproj,
    tail_input,
    tail_bproj,
    tail_cproj,
    step_bias,
    decay_log,
    block_input,
    block_bproj,
    block_step,
    lengths,
    state,
    gain_mix,
    w_out,
    gain_mlp,
    w_up,
    w_down,
):
    stream = inputs.astype(jnp.float32)
    squares = jnp.sum(stream * stream, axis=1)
    scaled = (stream * gain_in).astype(jnp.bfloat16)
    matrices = (w_gate, w_input, w_bproj, w_cproj, w_step)
    pieces = [jnp.dot(scaled, weight, preferred_element_type=jnp.float32) for weight in matrices]
    projected, totals = sent_together((jnp.concatenate(pieces, axis=1), squares), "kv", 0, 1)
    inverse = lax.rsqrt(totals / D + EPS)[:, None]
    bounds = [0]
    for weight in matrices:
        bounds.append(bounds[-1] + weight.shape[1])
    gate_pre, value_pre, b_pre, c_pre, step_pre = [
        projected[:, bounds[member] : bounds[member + 1]] * inverse for member in range(5)
    ]
    seq_count = lengths.shape[0]
    head_count = step_bias.shape[0]
    group_count = w_bproj.shape[1] // D_STATE
    block_len = block_step.shape[1]
    per_group = head_count // group_count
    current = convolve(tail_input, conv_input, value_pre)
    b_now = convolve(tail_bproj, conv_bproj, b_pre)
    c_now = convolve(tail_cproj, conv_cproj, c_pre)
    step_size = jax.nn.softplus(step_pre + step_bias)
    decay_rate = -jnp.exp(decay_log)
    positions = lax.broadcasted_iota(jnp.int32, (1, block_len), 1)
    live_rows = (positions < lengths[:, None]).astype(jnp.float32)
    masked = block_step * live_rows[:, :, None]
    later_steps = jnp.sum(masked, axis=1, keepdims=True) - jnp.cumsum(masked, axis=1)
    decays = jnp.exp(decay_rate * (step_size[:, None, :] + later_steps)) * live_rows[:, :, None]
    c_query = c_now.astype(jnp.bfloat16).reshape(seq_count, group_count, D_STATE)
    keys = block_bproj.reshape(seq_count, block_len, group_count, D_STATE)
    scores = jnp.einsum("bsgn,bgn->bsg", keys, c_query, preferred_element_type=jnp.float32)
    scores = jnp.repeat(scores, per_group, axis=2)
    weights = (decays * scores * block_step).astype(jnp.bfloat16)
    values = block_input.reshape(seq_count, block_len, head_count, HEAD_DIM)
    inner_sum = jnp.einsum("bsh,bshp->bhp", weights, values, preferred_element_type=jnp.float32)
    c_full = c_now.reshape(seq_count, group_count, D_STATE)
    b_full = b_now.reshape(seq_count, group_count, D_STATE)
    own_score = jnp.repeat(jnp.sum(c_full * b_full, axis=2), per_group, axis=1)
    own_term = (step_size * own_score)[:, :, None] * current.reshape(
        seq_count, head_count, HEAD_DIM
    )
    carried = jnp.exp(decay_rate * (step_size + jnp.sum(masked, axis=1)))
    c_heads = jnp.repeat(c_full, per_group, axis=1)
    readout = jnp.einsum("bhpn,bhn->bhp", state, c_heads, precision=lax.Precision.HIGHEST)
    mixed = (inner_sum + own_term + carried[:, :, None] * readout).reshape(
        seq_count, -1
    ) * jax.nn.silu(gate_pre)
    local_sq = jnp.sum(mixed * mixed, axis=1)
    total_sq = gathered_total(local_sq, "tp")
    normed = (mixed * lax.rsqrt(total_sq / SSM_WIDTH + EPS)[:, None] * gain_mix).astype(
        jnp.bfloat16
    )
    products = jnp.dot(gather_directly(normed, "kv", 0), w_out, preferred_element_type=jnp.float32)
    mixed_in = sent_and_summed(products, "tp", 1)
    column_count = mixed_in.shape[1]
    residual = lax.dynamic_slice_in_dim(
        stream, lax.axis_index("tp") * column_count, column_count, 1
    )
    hidden = (residual + mixed_in).astype(jnp.bfloat16)
    lifted = (hidden.astype(jnp.float32) * gain_mlp).astype(jnp.bfloat16)
    all_lifted, all_hidden = in_one_piece((lifted, hidden), "dp", 0, 1)
    whole_rows = all_hidden.astype(jnp.float32)
    row_sq = jnp.sum(whole_rows * whole_rows, axis=1)
    partial_value = jnp.dot(all_lifted, w_up, preferred_element_type=jnp.float32)
    sq_sum = of_everyone(row_sq, ("kv", "tp"))
    shares = summed_on_arrival(partial_value.astype(jnp.bfloat16), ("kv", "tp"), 1)
    unit_share = jnp.square(jax.nn.relu(shares * lax.rsqrt(sq_sum / D + EPS)[:, None])).astype(
        jnp.bfloat16
    )
    hidden_units = gathered_by_axis(unit_share, ("kv", "tp"), (0, 1), 1)
    lowered = sent_and_summed(
        jnp.dot(hidden_units, w_down, preferred_element_type=jnp.float32), "dp", 0
    )
    return (hidden.astype(jnp.float32) + lowered).astype(jnp.bfloat16)


def solution(mesh):
    return jax.shard_map(
        per_device,
        mesh=mesh,
        in_specs=(
            P(("grp", "dp"), "kv"),
            P("kv"),
            P("kv", "tp"),
            P("kv", "tp"),
            P("kv", "tp"),
            P("kv", "tp"),
            P("kv", "tp"),
            P(None, "tp"),
            P(None, "tp"),
            P(None, "tp"),
            P(("grp", "dp", "kv"), None, "tp"),
            P(("grp", "dp", "kv"), None, "tp"),
            P(("grp", "dp", "kv"), None, "tp"),
            P("tp"),
            P("tp"),
            P(("grp", "dp", "kv"), None, "tp"),
            P(("grp", "dp", "kv"), None, "tp"),
            P(("grp", "dp", "kv"), None, "tp"),
            P(("grp", "dp", "kv")),
            P(("grp", "dp", "kv"), "tp", None, None),
            P("tp"),
            P("tp", "kv"),
            P(("kv", "tp")),
            P(("kv", "tp"), "dp"),
            P("dp", ("kv", "tp")),
        ),
        out_specs=P(("grp", "dp"), ("kv", "tp")),
        check_vma=False,
    )
```

profile of v0, /device:TPU:65, one launch (start us, length us, event | category | flops | bytes accessed | tf_op | source)
XLA Modules:
  0.0 298.7 jit_solution(5687502616347760678)
XLA Ops:
  6.6 0.9 multiply_reduce_fusion.1
  7.5 0.1 concatenate.27
  7.6 0.9 fusion.14
  8.5 1.1 fusion.16
  9.7 1.2 fusion.15
  10.9 1.3 fusion.18
  12.2 0.1 concatenate.19
  12.3 0.9 fusion.17
  13.3 0.1 concatenate.20
  13.4 1.2 concatenate.25
  14.6 44.4 %all-to-all-start = ((f32[16,2,3089]{2,1,0:T(2,128)}), f32[16,2,3089]{2,1,0:T(2,128)S(1)}, u32[]{:S(2)}, u32[]{:S(2)}) async-start(f32[16,2,3089]{2,1,0:T(2,128)} %concatenate.25), calls=%async_computation | async-start | bytes 819200 | tf_op jit(solution)/shard_map/all_to_all | solution.py:22
  59.0 0.1 copy.71
  59.1 0.2 copy.88
  59.3 1.0 copy.74
  60.3 1.3 dynamic-slice
  62.3 0.1 fusion.33
  62.4 0.2 reduce_window_sum.11
  62.7 15.6 %all-to-all-done = f32[16,2,3089]{2,1,0:T(2,128)S(1)} async-done(((f32[16,2,3089]{2,1,0:T(2,128)}), f32[16,2,3089]{2,1,0:T(2,128)S(1)}, u32[]{:S(2)}, u32[]{:S(2)}) %all-to-all-start) | async-done | bytes 395424 | tf_op jit(solution)/shard_map/all_to_all | solution.py:22
  78.3 0.1 reduce_sum.106
  78.5 0.2 fusion.30
  78.7 0.1 fusion.34
  78.8 0.1 multiply_reduce_fusion.3
  78.9 0.1 broadcast_in_dim.11
  79.0 0.1 reshape.166
  79.1 0.1 divide_multiply_fusion.1
  79.2 0.1 reshape.167
  79.2 0.2 fusion.38
  79.4 0.1 copy.72
  79.5 0.1 fusion.32
  79.6 0.1 fusion.2
  79.8 0.1 copy.84
  79.9 1.7 fusion.40
  81.6 1.4 fusion.39
  83.0 0.1 multiply_add_fusion
  83.1 0.1 reshape.169
  83.2 0.2 multiply_reduce_fusion.2
  83.4 0.2 dynamic-update-slice
  83.7 8.0 %all-reduce = f32[4]{0:T(128)S(1)} all-reduce(f32[4]{0:T(128)S(1)} %dynamic-update-slice), channel_id=2, replica_groups=mesh['grp'=2,'dp'=8,'kv'=16,'tp'=2] {'tp'}, use_global_device_ids=true, to_apply=%add | all-reduce | flops 4 | bytes 32
  91.6 0.1 reshape.183
  91.8 0.1 multiply_convert_fusion.2
  91.8 0.7 broadcast_in_dim.13
  92.5 6.0 %all-to-all-start.1 = ((bf16[16,2,1024]{2,1,0:T(2,128)(2,1)}), bf16[16,2,1024]{2,1,0:T(2,128)(2,1)S(1)}, u32[]{:S(2)}, u32[]{:S(2)}) async-start(bf16[16,2,1024]{2,1,0:T(2,128)(2,1)} %broadcast_in_dim.13), calls=%async_computation.1 | async-start | bytes 131072 | tf_op jit(solution)/shard_map/all_to_all | solution.py:42
  98.5 0.2 copy.89
  98.7 11.2 %all-to-all-done.1 = bf16[16,2,1024]{2,1,0:T(2,128)(2,1)S(1)} async-done(((bf16[16,2,1024]{2,1,0:T(2,128)(2,1)}), bf16[16,2,1024]{2,1,0:T(2,128)(2,1)S(1)}, u32[]{:S(2)}, u32[]{:S(2)}) %all-to-all-start.1) | async-done | bytes 65568 | tf_op jit(solution)/shard_map/all_to_all | solution.py:42
  110.0 0.2 convolution_bitcast_fusion
  110.2 5.5 %all_to_all.31 = f32[2,32,128]{2,1,0:T(8,128)S(1)} all-to-all(f32[2,32,128]{2,1,0:T(8,128)S(1)} %convolution_bitcast_fusion), channel_id=1, replica_groups=mesh['grp'=2,'dp'=8,'kv'=16,'tp'=2] {'tp'}, dimensions={0} | all-to-all | bytes 65536 | tf_op jit(solution)/shard_map/all_to_all | solution.py:22
  115.7 20.2 %all_gather.17 = bf16[256,256]{1,0:T(8,128)(2,1)S(1)} all-gather(bf16[32,256]{1,0:T(8,128)(2,1)S(1)} %pad_maximum_fusion), channel_id=1, replica_groups=mesh['grp'=2,'dp'=8,'kv'=16,'tp'=2] {'dp'}, dimensions={0}, use_global_device_ids=true | all-gather | bytes 147456 | tf_op jit(solution)/shard_map/all_gather | solution.py:64
  135.9 0.1 multiply_reduce_fusion
  136.0 0.6 broadcast_in_dim.14
  136.6 10.4 %all-to-all-start.4 = ((f32[32,1,256]{2,1,0:T(1,128)}), f32[32,1,256]{2,1,0:T(1,128)S(1)}, u32[]{:S(2)}, u32[]{:S(2)}) async-start(f32[32,1,256]{2,1,0:T(1,128)} %broadcast_in_dim.14), calls=%async_computation.4 | async-start | bytes 65536 | tf_op jit(solution)/shard_map/all_to_all | solution.py:42
  147.1 0.4 convolution_convert_fusion
  147.5 1.3 copy.76
  148.8 10.4 %all-to-all-done.4 = f32[32,1,256]{2,1,0:T(1,128)S(1)} async-done(((f32[32,1,256]{2,1,0:T(1,128)}), f32[32,1,256]{2,1,0:T(1,128)S(1)}, u32[]{:S(2)}, u32[]{:S(2)}) %all-to-all-start.4) | async-done | bytes 32800 | tf_op jit(solution)/shard_map/all_to_all | solution.py:42
  159.2 4.8 %all-to-all-start.3 = ((bf16[32,256,64]{1,2,0:T(8,128)(2,1)}), bf16[32,256,64]{1,2,0:T(8,128)(2,1)S(1)}, u32[]{:S(2)}, u32[]{:S(2)}) async-start(bf16[32,256,64]{1,2,0:T(8,128)(2,1)} %bitcast.41), calls=%async_computation.3 | async-start | bytes 2097152 | tf_op jit(solution)/shard_map/all_to_all | solution.py:74
  164.2 55.5 %all-to-all-done.3 = bf16[32,256,64]{1,2,0:T(8,128)(2,1)S(1)} async-done(((bf16[32,256,64]{1,2,0:T(8,128)(2,1)}), bf16[32,256,64]{1,2,0:T(8,128)(2,1)S(1)}, u32[]{:S(2)}, u32[]{:S(2)}) %all-to-all-start.3) | async-done | bytes 1048608 | tf_op jit(solution)/shard_map/all_to_all | solution.py:74
  219.7 0.2 convert_reduce_fusion
  219.8 24.8 %all_gather.18 = bf16[16,256,64]{1,2,0:T(8,128)(2,1)} all-gather(bf16[1,256,64]{1,2,0:T(8,128)(2,1)S(1)} %fusion.6), channel_id=1, replica_groups=mesh['grp'=2,'dp'=8,'kv'=16,'tp'=2] {'kv'}, dimensions={0}, use_global_device_ids=true | all-gather | bytes 557056 | tf_op jit(solution)/shard_map/all_gather | solution.py:81
  244.7 23.7 %all-gather.3.cloned.1.call-done = bf16[32,256,64]{1,2,0:T(8,128)(2,1)} async-done(((bf16[16,256,64]{1,2,0:T(8,128)(2,1)}), bf16[32,256,64]{1,2,0:T(8,128)(2,1)}) %all-gather.3.cloned.1.call-update) | async-done | bytes 1048592 | tf_op jit(solution)/shard_map/all_gather | solution.py:81
  268.5 2.4 copy.78
  270.8 3.9 %copy.79 = bf16[256,32,64]{2,1,0:T(8,128)(2,1)S(1)} copy(bf16[256,32,64]{0,2,1:T(8,128)(2,1)} %bitcast.101) | data formatting | bytes 2097152 | tf_op jit(solution)/shard_map/transpose | solution.py:50
  274.7 2.4 dot_general.51
  277.2 1.8 fusion
  279.0 12.3 %all_to_all.32 = f32[8,32,128]{2,1,0:T(8,128)S(1)} all-to-all(f32[8,32,128]{2,1,0:T(8,128)S(1)} %fusion), channel_id=1, replica_groups=mesh['grp'=2,'dp'=8,'kv'=16,'tp'=2] {'dp'}, dimensions={0} | all-to-all | bytes 262144 | tf_op jit(solution)/shard_map/all_to_all | solution.py:22
  291.3 0.6 fusion.8
  (65 shorter events, 0.7 us)
Async XLA Ops:
  6.5 73.3 %copy-start = (f32[2,16,64,128]{3,2,1,0:T(8,128)S(1)}, f32[2,16,64,128]{3,2,1,0:T(8,128)}, u32[]{:S(2)}) copy-start(f32[2,16,64,128]{3,2,1,0:T(8,128)} %param.44) | copy-start | bytes 3145732
  6.6 5.8 %copy-start.3 = (bf16[256,1024]{1,0:T(8,128)(2,1)S(1)}, bf16[256,1024]{1,0:T(8,128)(2,1)}, u32[]{:S(2)}) copy-start(bf16[256,1024]{1,0:T(8,128)(2,1)} %param.28) | copy-start | bytes 1572868
  9.6 49.4 %copy-start.7 = (f32[2,128,16]{1,2,0:T(8,128)S(1)}, f32[2,128,16]{1,2,0:T(8,128)}, u32[]{:S(2)}) copy-start(f32[2,128,16]{1,2,0:T(8,128)} %param.42) | copy-start | bytes 49156
  9.7 49.4 %copy-start.6 = (bf16[2,128,512]{2,1,0:T(8,128)(2,1)S(1)}, bf16[2,128,512]{2,1,0:T(8,128)(2,1)}, u32[]{:S(2)}) copy-start(bf16[2,128,512]{2,1,0:T(8,128)(2,1)} %param.41) | copy-start | bytes 786436
  10.9 48.4 %copy-start.4 = (bf16[2,128,1024]{2,1,0:T(8,128)(2,1)S(1)}, bf16[2,128,1024]{2,1,0:T(8,128)(2,1)}, u32[]{:S(2)}) copy-start(bf16[2,128,1024]{2,1,0:T(8,128)(2,1)} %param.40) | copy-start | bytes 1572868
  12.3 49.9 %copy-start.17 = (s32[2]{0:T(128)S(1)}, s32[2]{0:T(128)}, u32[]{:S(2)}) copy-start(s32[2]{0:T(128)} %param.43) | copy-start | bytes 28
  13.3 49.3 %copy-start.18 = (f32[16]{0:T(128)S(1)}, f32[16]{0:T(128)}, u32[]{:S(2)}) copy-start(f32[16]{0:T(128)} %param.39) | copy-start | bytes 196
  13.3 49.3 %copy-start.10 = (f32[4,512]{1,0:T(4,128)S(1)}, f32[4,512]{1,0:T(4,128)}, u32[]{:S(2)}) copy-start(f32[4,512]{1,0:T(4,128)} %param.33) | copy-start | bytes 24580
  13.3 49.3 %copy-start.11 = (f32[4,512]{1,0:T(4,128)S(1)}, f32[4,512]{1,0:T(4,128)}, u32[]{:S(2)}) copy-start(f32[4,512]{1,0:T(4,128)} %param.34) | copy-start | bytes 24580
  13.3 49.3 %copy-start.8 = (f32[4,1024]{1,0:T(4,128)S(1)}, f32[4,1024]{1,0:T(4,128)}, u32[]{:S(2)}) copy-start(f32[4,1024]{1,0:T(4,128)} %param.32) | copy-start | bytes 49156
  13.4 65.2 %copy-start.12 = (bf16[2,3,512]{2,0,1:T(2,128)(2,1)S(1)}, bf16[2,3,512]{2,0,1:T(2,128)(2,1)}, u32[]{:S(2)}) copy-start(bf16[2,3,512]{2,0,1:T(2,128)(2,1)} %param.37) | copy-start | bytes 18436
  13.4 65.2 %copy-start.13 = (bf16[2,3,512]{2,0,1:T(2,128)(2,1)S(1)}, bf16[2,3,512]{2,0,1:T(2,128)(2,1)}, u32[]{:S(2)}) copy-start(bf16[2,3,512]{2,0,1:T(2,128)(2,1)} %param.36) | copy-start | bytes 18436
  13.4 65.6 %copy-start.9 = (bf16[2,3,1024]{2,0,1:T(2,128)(2,1)S(1)}, bf16[2,3,1024]{2,0,1:T(2,128)(2,1)}, u32[]{:S(2)}) copy-start(bf16[2,3,1024]{2,0,1:T(2,128)(2,1)} %param.35) | copy-start | bytes 36868
  14.6 64.9 %copy-start.16 = (f32[16]{0:T(128)S(1)}, f32[16]{0:T(128)}, u32[]{:S(2)}) copy-start(f32[16]{0:T(128)} %param.38) | copy-start | bytes 196
  14.6 63.7 %all-to-all-start = ((f32[16,2,3089]{2,1,0:T(2,128)}), f32[16,2,3089]{2,1,0:T(2,128)S(1)}, u32[]{:S(2)}, u32[]{:S(2)}) async-start(f32[16,2,3089]{2,1,0:T(2,128)} %concatenate.25), calls=%async_computation | async-start | bytes 819200 | tf_op jit(solution)/shard_map/all_to_all | solution.py:22
  60.3 31.5 %copy-start.14 = (f32[1024]{0:T(1024)S(1)}, f32[1024]{0:T(1024)}, u32[]{:S(2)}) copy-start(f32[1024]{0:T(1024)} %param.45) | copy-start | bytes 12292
  62.3 36.2 %copy-start.1 = (bf16[32,256]{1,0:T(8,128)(2,1)S(1)}, bf16[32,256]{1,0:T(8,128)(2,1)}, u32[]{:S(2)}) copy-start(bf16[32,256]{1,0:T(8,128)(2,1)} %param.25) | copy-start | bytes 49156
  62.4 36.1 %copy-start.5 = (bf16[1024,256]{1,0:T(8,128)(2,1)S(1)}, bf16[1024,256]{1,0:T(8,128)(2,1)}, u32[]{:S(2)}) copy-start(bf16[1024,256]{1,0:T(8,128)(2,1)} %param.46) | copy-start | bytes 1572868
  79.8 35.9 %copy-start.15 = (f32[128]{0:T(128)S(1)}, f32[128]{0:T(128)}, u32[]{:S(2)}) copy-start(f32[128]{0:T(128)} %param.47) | copy-start | bytes 1540
  79.9 67.2 %copy-start.2 = (bf16[128,2048]{1,0:T(8,128)(2,1)S(1)}, bf16[128,2048]{1,0:T(8,128)(2,1)}, u32[]{:S(2)}) copy-start(bf16[128,2048]{1,0:T(8,128)(2,1)} %param.48) | copy-start | bytes 1572868
  92.5 17.4 %all-to-all-start.1 = ((bf16[16,2,1024]{2,1,0:T(2,128)(2,1)}), bf16[16,2,1024]{2,1,0:T(2,128)(2,1)S(1)}, u32[]{:S(2)}, u32[]{:S(2)}) async-start(bf16[16,2,1024]{2,1,0:T(2,128)(2,1)} %broadcast_in_dim.13), calls=%async_computation.1 | async-start | bytes 131072 | tf_op jit(solution)/shard_map/all_to_all | solution.py:42
  136.6 22.6 %all-to-all-start.4 = ((f32[32,1,256]{2,1,0:T(1,128)}), f32[32,1,256]{2,1,0:T(1,128)S(1)}, u32[]{:S(2)}, u32[]{:S(2)}) async-start(f32[32,1,256]{2,1,0:T(1,128)} %broadcast_in_dim.14), calls=%async_computation.4 | async-start | bytes 65536 | tf_op jit(solution)/shard_map/all_to_all | solution.py:42
  159.2 60.5 %all-to-all-start.3 = ((bf16[32,256,64]{1,2,0:T(8,128)(2,1)}), bf16[32,256,64]{1,2,0:T(8,128)(2,1)S(1)}, u32[]{:S(2)}, u32[]{:S(2)}) async-start(bf16[32,256,64]{1,2,0:T(8,128)(2,1)} %bitcast.41), calls=%async_computation.3 | async-start | bytes 2097152 | tf_op jit(solution)/shard_map/all_to_all | solution.py:74
  164.1 104.4 %all-gather.3.cloned.1.call-start = ((), (), s32[]{:S(2)}) async-start(), calls=%async_computation.6 | async-start | bytes 1572864 | tf_op jit(solution)/shard_map/all_gather | solution.py:81
Sparse Core Ops, SparseCore 0:
  244.8 23.5 all-gather.2
where the time goes:
time: 300 us; the launch traced here: 299 us
  waiting for transfers between devices  117 us (39%)
  blocking collectives  70.7 us (24%)
  starting transfers between devices  65.6 us (22%)
  local copies, waits for them, and re-layouts  16.7 us (6%)
  between operations  14.5 us (5%)
  matrix products  11.2 us (4%)
  other arithmetic  3.49 us (1%)
    all_to_all x1, waiting for transfers between devices, summed_on_arrival(): lax.all_to_all(tiles, axis, split_axis=0, concat_axis=0, tiled=True)  55.5 us
    all_to_all x1, starting transfers between devices, sent_and_summed(): tiles = lax.all_to_all(in_blocks(shard, dim, size), axis, 0, 0, tiled=True)  44.4 us
    all_gather x1, blocking collectives, stacked_from(): tiles = lax.all_gather(tiles, axes[k], axis=0, tiled=True)  24.8 us
    all_gather x1, waiting for transfers between devices, stacked_from(): tiles = lax.all_gather(tiles, axes[k], axis=0, tiled=True)  23.7 us
    all_to_all x2, waiting for transfers between devices, from_everyone(): lax.all_to_all(jnp.broadcast_to(shard[None], (size, *shard.shape)), axis,...  21.6 us
    all_gather x1, blocking collectives, in_one_piece(): lax.all_gather(both, axis, axis=dim, tiled=True)  20.2 us
    all_to_all x2, blocking collectives, sent_and_summed(): tiles = lax.all_to_all(in_blocks(shard, dim, size), axis, 0, 0, tiled=True)  17.7 us
    all_to_all x2, starting transfers between devices, from_everyone(): lax.all_to_all(jnp.broadcast_to(shard[None], (size, *shard.shape)), axis,...  16.4 us
  transfers between devices with their start and end apart: 5, of which 5 were waited for; matrix products, arithmetic and copies ran while one was open for 2% of the time, Pallas kernels for 0%

commit v1 on v0

--- a/solution.py
+++ b/solution.py
@@ -78,7 +78,16 @@
 def stacked_from(shard, axes, order):
     tiles = shard[None]
     for k in order:
-        tiles = lax.all_gather(tiles, axes[k], axis=0, tiled=True)
+        meet_figure = lambda peer_axis, array_here: jnp.concatenate(
+            lax.all_to_all(
+                jnp.stack([array_here for _ in range(lax.axis_size(peer_axis))], axis=0),
+                axis_name=peer_axis,
+                split_axis=0,
+                concat_axis=0,
+            ),
+            axis=0,
+        )
+        tiles = meet_figure(axes[k], tiles)
     current = [lax.axis_size(axes[k]) for k in reversed(order)]
     tiles = tiles.reshape(*current, *shard.shape)
     turned = sorted(range(len(order)), key=lambda place: order[len(order) - 1 - place])

time: 300 us -> 274 us (0.913)
  waiting for transfers between devices: 117 us -> 92.7 us
  between operations: 14.5 us -> 1.14 us
  blocking collectives: 70.7 us -> 83.7 us
    all_to_all x0 -> x2, blocking collectives: none -> 37.1 us  [stacked_from(): lax.all_to_all(jnp.stack([array_here for _ in range(lax.axis_size(peer_ax...]
    all_gather x1 -> x0, blocking collectives: 24.8 us -> none  [stacked_from(): tiles = lax.all_gather(tiles, axes[k], axis=0, tiled=True)]
    all_gather x1 -> x0, waiting for transfers between devices: 23.7 us -> none  [stacked_from(): tiles = lax.all_gather(tiles, axes[k], axis=0, tiled=True)]
  transfers between devices with their start and end apart: 5 -> 4, of which waited for: 5 -> 4; matrix products, arithmetic and copies ran while one was open for 2% -> 2% of each run, Pallas kernels for 0% -> 0%
where the time goes in v1:
time: 274 us; the launch traced here: 272 us
  waiting for transfers between devices  92.7 us (34%)
  blocking collectives  83.7 us (31%)
  starting transfers between devices  65.6 us (24%)
  local copies, waits for them, and re-layouts  15.4 us (6%)
  matrix products  10.1 us (4%)
  other arithmetic  3.58 us (1%)
    all_to_all x1, waiting for transfers between devices, summed_on_arrival(): lax.all_to_all(tiles, axis, split_axis=0, concat_axis=0, tiled=True)  55.5 us
    all_to_all x1, starting transfers between devices, sent_and_summed(): tiles = lax.all_to_all(in_blocks(shard, dim, size), axis, 0, 0, tiled=True)  44.4 us
    all_to_all x2, blocking collectives, stacked_from(): lax.all_to_all(jnp.stack([array_here for _ in range(lax.axis_size(peer_ax...  37.1 us
    all_to_all x2, waiting for transfers between devices, from_everyone(): lax.all_to_all(jnp.broadcast_to(shard[None], (size, *shard.shape)), axis,...  21.6 us
    all_gather x1, blocking collectives, in_one_piece(): lax.all_gather(both, axis, axis=dim, tiled=True)  20.2 us
    all_to_all x2, blocking collectives, sent_and_summed(): tiles = lax.all_to_all(in_blocks(shard, dim, size), axis, 0, 0, tiled=True)  18.4 us
    all_to_all x2, starting transfers between devices, from_everyone(): lax.all_to_all(jnp.broadcast_to(shard[None], (size, *shard.shape)), axis,...  16.4 us
    all_to_all x1, waiting for transfers between devices, sent_and_summed(): tiles = lax.all_to_all(in_blocks(shard, dim, size), axis, 0, 0, tiled=True)  15.6 us
  transfers between devices with their start and end apart: 4, of which 4 were waited for; matrix products, arithmetic and copies ran while one was open for 2% of the time, Pallas kernels for 0%

profile of v1, /device:TPU:65, one launch (start us, length us, event | category | flops | bytes accessed | tf_op | source)
XLA Modules:
  0.0 272.3 jit_solution(15488241670120172030)
XLA Ops:
  0.0 0.9 multiply_reduce_fusion.1
  1.0 0.1 concatenate.27
  1.1 0.9 fusion.11
  1.9 1.1 fusion.13
  3.1 1.2 fusion.12
  4.4 1.3 fusion.15
  5.7 0.1 concatenate.19
  5.8 0.9 fusion.14
  6.8 0.1 concatenate.20
  6.9 1.2 concatenate.25
  8.0 44.4 %all-to-all-start = ((f32[16,2,3089]{2,1,0:T(2,128)}), f32[16,2,3089]{2,1,0:T(2,128)S(1)}, u32[]{:S(2)}, u32[]{:S(2)}) async-start(f32[16,2,3089]{2,1,0:T(2,128)} %concatenate.25), calls=%async_computation | async-start | bytes 819200 | tf_op jit(solution)/shard_map/all_to_all | solution.py:22
  52.4 0.1 copy.61
  52.5 0.2 copy.78
  52.7 1.0 copy.64
  53.7 1.3 dynamic-slice
  55.8 0.1 fusion.30
  55.9 0.2 reduce_window_sum.11
  56.2 15.6 %all-to-all-done = f32[16,2,3089]{2,1,0:T(2,128)S(1)} async-done(((f32[16,2,3089]{2,1,0:T(2,128)}), f32[16,2,3089]{2,1,0:T(2,128)S(1)}, u32[]{:S(2)}, u32[]{:S(2)}) %all-to-all-start) | async-done | bytes 395424 | tf_op jit(solution)/shard_map/all_to_all | solution.py:22
  71.8 0.1 reduce_sum.104
  71.9 0.2 fusion.27
  72.1 0.1 fusion.31
  72.3 0.1 multiply_reduce_fusion.3
  72.4 0.1 reshape.150
  72.5 0.1 divide_multiply_fusion.1
  72.6 0.1 reshape.151
  72.7 0.2 fusion.35
  72.9 0.1 copy.62
  73.0 0.1 fusion.29
  73.1 0.1 fusion.2
  73.2 0.1 copy.74
  73.3 1.7 fusion.37
  75.1 0.4 fusion.36
  75.5 0.1 multiply_add_fusion
  75.5 0.1 reshape.153
  75.6 0.2 multiply_reduce_fusion.2
  75.8 0.2 dynamic-update-slice
  76.1 8.0 %all-reduce = f32[4]{0:T(128)S(1)} all-reduce(f32[4]{0:T(128)S(1)} %dynamic-update-slice), channel_id=2, replica_groups=mesh['grp'=2,'dp'=8,'kv'=16,'tp'=2] {'tp'}, use_global_device_ids=true, to_apply=%add | all-reduce | flops 4 | bytes 32
  84.0 0.1 reshape.166
  84.2 0.1 multiply_convert_fusion.3
  84.2 0.7 broadcast_in_dim.13
  84.9 6.0 %all-to-all-start.1 = ((bf16[16,2,1024]{2,1,0:T(2,128)(2,1)}), bf16[16,2,1024]{2,1,0:T(2,128)(2,1)S(1)}, u32[]{:S(2)}, u32[]{:S(2)}) async-start(bf16[16,2,1024]{2,1,0:T(2,128)(2,1)} %broadcast_in_dim.13), calls=%async_computation.1 | async-start | bytes 131072 | tf_op jit(solution)/shard_map/all_to_all | solution.py:42
  90.9 0.2 copy.79
  91.1 11.2 %all-to-all-done.1 = bf16[16,2,1024]{2,1,0:T(2,128)(2,1)S(1)} async-done(((bf16[16,2,1024]{2,1,0:T(2,128)(2,1)}), bf16[16,2,1024]{2,1,0:T(2,128)(2,1)S(1)}, u32[]{:S(2)}, u32[]{:S(2)}) %all-to-all-start.1) | async-done | bytes 65568 | tf_op jit(solution)/shard_map/all_to_all | solution.py:42
  102.4 0.2 convolution_bitcast_fusion
  102.6 5.5 %all_to_all.41 = f32[2,32,128]{2,1,0:T(8,128)S(1)} all-to-all(f32[2,32,128]{2,1,0:T(8,128)S(1)} %convolution_bitcast_fusion), channel_id=1, replica_groups=mesh['grp'=2,'dp'=8,'kv'=16,'tp'=2] {'tp'}, dimensions={0} | all-to-all | bytes 65536 | tf_op jit(solution)/shard_map/all_to_all | solution.py:22
  108.1 20.2 %all_gather.11 = bf16[256,256]{1,0:T(8,128)(2,1)S(1)} all-gather(bf16[32,256]{1,0:T(8,128)(2,1)S(1)} %pad_maximum_fusion.1), channel_id=1, replica_groups=mesh['grp'=2,'dp'=8,'kv'=16,'tp'=2] {'dp'}, dimensions={0}, use_global_device_ids=true | all-gather | bytes 147456 | tf_op jit(solution)/shard_map/all_gather | solution.py:64
  128.3 0.1 multiply_reduce_fusion
  128.4 0.6 broadcast_in_dim.14
  129.1 10.4 %all-to-all-start.4 = ((f32[32,1,256]{2,1,0:T(1,128)}), f32[32,1,256]{2,1,0:T(1,128)S(1)}, u32[]{:S(2)}, u32[]{:S(2)}) async-start(f32[32,1,256]{2,1,0:T(1,128)} %broadcast_in_dim.14), calls=%async_computation.4 | async-start | bytes 65536 | tf_op jit(solution)/shard_map/all_to_all | solution.py:42
  139.5 0.4 convolution_convert_fusion
  139.9 1.3 copy.66
  141.2 10.4 %all-to-all-done.4 = f32[32,1,256]{2,1,0:T(1,128)S(1)} async-done(((f32[32,1,256]{2,1,0:T(1,128)}), f32[32,1,256]{2,1,0:T(1,128)S(1)}, u32[]{:S(2)}, u32[]{:S(2)}) %all-to-all-start.4) | async-done | bytes 32800 | tf_op jit(solution)/shard_map/all_to_all | solution.py:42
  151.6 4.8 %all-to-all-start.3 = ((bf16[32,256,64]{1,2,0:T(8,128)(2,1)}), bf16[32,256,64]{1,2,0:T(8,128)(2,1)S(1)}, u32[]{:S(2)}, u32[]{:S(2)}) async-start(bf16[32,256,64]{1,2,0:T(8,128)(2,1)} %bitcast.41), calls=%async_computation.3 | async-start | bytes 2097152 | tf_op jit(solution)/shard_map/all_to_all | solution.py:74
  156.5 55.5 %all-to-all-done.3 = bf16[32,256,64]{1,2,0:T(8,128)(2,1)S(1)} async-done(((bf16[32,256,64]{1,2,0:T(8,128)(2,1)}), bf16[32,256,64]{1,2,0:T(8,128)(2,1)S(1)}, u32[]{:S(2)}, u32[]{:S(2)}) %all-to-all-start.3) | async-done | bytes 1048608 | tf_op jit(solution)/shard_map/all_to_all | solution.py:74
  212.1 0.2 convert_reduce_fusion
  212.3 26.1 %all_to_all.42 = bf16[16,1,256,64]{2,3,1,0:T(8,128)(2,1)S(1)} all-to-all(bf16[16,1,256,64]{2,3,1,0:T(8,128)(2,1)S(1)} %stack.6), channel_id=1, replica_groups=mesh['grp'=2,'dp'=8,'kv'=16,'tp'=2] {'kv'}, dimensions={0} | all-to-all | bytes 1048576 | tf_op jit(solution)/shard_map/all_to_all | solution.py:82
  238.4 0.1 pad_maximum_fusion
  238.5 11.0 %all_to_all.43 = bf16[2,16,256,64]{2,3,1,0:T(8,128)(2,1)S(1)} all-to-all(bf16[2,16,256,64]{2,3,1,0:T(8,128)(2,1)S(1)} %pad_maximum_fusion), channel_id=1, replica_groups=mesh['grp'=2,'dp'=8,'kv'=16,'tp'=2] {'tp'}, dimensions={0} | all-to-all | bytes 2097152 | tf_op jit(solution)/shard_map/all_to_all | solution.py:82
  249.5 1.1 copy.68
  250.5 3.9 %copy.69 = bf16[256,32,64]{2,1,0:T(8,128)(2,1)S(1)} copy(bf16[256,32,64]{0,2,1:T(8,128)(2,1)} %bitcast.92) | data formatting | bytes 2097152 | tf_op jit(solution)/shard_map/transpose | solution.py:50
  254.5 2.4 dot_general.51
  256.9 1.8 fusion
  258.7 13.0 %all_to_all.44 = f32[8,32,128]{2,1,0:T(8,128)S(1)} all-to-all(f32[8,32,128]{2,1,0:T(8,128)S(1)} %fusion), channel_id=1, replica_groups=mesh['grp'=2,'dp'=8,'kv'=16,'tp'=2] {'dp'}, dimensions={0} | all-to-all | bytes 262144 | tf_op jit(solution)/shard_map/all_to_all | solution.py:22
  271.7 0.6 fusion.5
  (67 shorter events, 0.7 us)
Async XLA Ops:
  0.0 73.3 %copy-start = (f32[2,16,64,128]{3,2,1,0:T(8,128)S(1)}, f32[2,16,64,128]{3,2,1,0:T(8,128)}, u32[]{:S(2)}) copy-start(f32[2,16,64,128]{3,2,1,0:T(8,128)} %param.44) | copy-start | bytes 3145732
  0.0 5.8 %copy-start.3 = (bf16[256,1024]{1,0:T(8,128)(2,1)S(1)}, bf16[256,1024]{1,0:T(8,128)(2,1)}, u32[]{:S(2)}) copy-start(bf16[256,1024]{1,0:T(8,128)(2,1)} %param.28) | copy-start | bytes 1572868
  3.1 49.4 %copy-start.8 = (f32[2,128,16]{1,2,0:T(8,128)S(1)}, f32[2,128,16]{1,2,0:T(8,128)}, u32[]{:S(2)}) copy-start(f32[2,128,16]{1,2,0:T(8,128)} %param.42) | copy-start | bytes 49156
  3.1 49.4 %copy-start.7 = (bf16[2,128,512]{2,1,0:T(8,128)(2,1)S(1)}, bf16[2,128,512]{2,1,0:T(8,128)(2,1)}, u32[]{:S(2)}) copy-start(bf16[2,128,512]{2,1,0:T(8,128)(2,1)} %param.41) | copy-start | bytes 786436
  4.3 48.4 %copy-start.4 = (bf16[2,128,1024]{2,1,0:T(8,128)(2,1)S(1)}, bf16[2,128,1024]{2,1,0:T(8,128)(2,1)}, u32[]{:S(2)}) copy-start(bf16[2,128,1024]{2,1,0:T(8,128)(2,1)} %param.40) | copy-start | bytes 1572868
  5.8 49.9 %copy-start.18 = (s32[2]{0:T(128)S(1)}, s32[2]{0:T(128)}, u32[]{:S(2)}) copy-start(s32[2]{0:T(128)} %param.43) | copy-start | bytes 28
  6.7 49.4 %copy-start.19 = (f32[16]{0:T(128)S(1)}, f32[16]{0:T(128)}, u32[]{:S(2)}) copy-start(f32[16]{0:T(128)} %param.39) | copy-start | bytes 196
  6.7 49.4 %copy-start.11 = (f32[4,512]{1,0:T(4,128)S(1)}, f32[4,512]{1,0:T(4,128)}, u32[]{:S(2)}) copy-start(f32[4,512]{1,0:T(4,128)} %param.33) | copy-start | bytes 24580
  6.7 49.4 %copy-start.12 = (f32[4,512]{1,0:T(4,128)S(1)}, f32[4,512]{1,0:T(4,128)}, u32[]{:S(2)}) copy-start(f32[4,512]{1,0:T(4,128)} %param.34) | copy-start | bytes 24580
  6.8 49.4 %copy-start.9 = (f32[4,1024]{1,0:T(4,128)S(1)}, f32[4,1024]{1,0:T(4,128)}, u32[]{:S(2)}) copy-start(f32[4,1024]{1,0:T(4,128)} %param.32) | copy-start | bytes 49156
  6.8 65.2 %copy-start.13 = (bf16[2,3,512]{2,0,1:T(2,128)(2,1)S(1)}, bf16[2,3,512]{2,0,1:T(2,128)(2,1)}, u32[]{:S(2)}) copy-start(bf16[2,3,512]{2,0,1:T(2,128)(2,1)} %param.37) | copy-start | bytes 18436
  6.9 65.2 %copy-start.14 = (bf16[2,3,512]{2,0,1:T(2,128)(2,1)S(1)}, bf16[2,3,512]{2,0,1:T(2,128)(2,1)}, u32[]{:S(2)}) copy-start(bf16[2,3,512]{2,0,1:T(2,128)(2,1)} %param.36) | copy-start | bytes 18436
  6.9 65.6 %copy-start.10 = (bf16[2,3,1024]{2,0,1:T(2,128)(2,1)S(1)}, bf16[2,3,1024]{2,0,1:T(2,128)(2,1)}, u32[]{:S(2)}) copy-start(bf16[2,3,1024]{2,0,1:T(2,128)(2,1)} %param.35) | copy-start | bytes 36868
  8.0 64.9 %copy-start.17 = (f32[16]{0:T(128)S(1)}, f32[16]{0:T(128)}, u32[]{:S(2)}) copy-start(f32[16]{0:T(128)} %param.38) | copy-start | bytes 196
  8.0 63.7 %all-to-all-start = ((f32[16,2,3089]{2,1,0:T(2,128)}), f32[16,2,3089]{2,1,0:T(2,128)S(1)}, u32[]{:S(2)}, u32[]{:S(2)}) async-start(f32[16,2,3089]{2,1,0:T(2,128)} %concatenate.25), calls=%async_computation | async-start | bytes 819200 | tf_op jit(solution)/shard_map/all_to_all | solution.py:22
  53.7 21.4 %copy-start.6 = (bf16[2,128,1024]{1,2,0:T(8,128)(2,1)S(1)}, bf16[2,128,1024]{1,2,0:T(8,128)(2,1)}, u32[]{:S(2)}) copy-start(bf16[2,128,1024]{1,2,0:T(8,128)(2,1)} %copy.64) | copy-start | bytes 1572868
  53.7 30.5 %copy-start.15 = (f32[1024]{0:T(1024)S(1)}, f32[1024]{0:T(1024)}, u32[]{:S(2)}) copy-start(f32[1024]{0:T(1024)} %param.45) | copy-start | bytes 12292
  55.8 35.1 %copy-start.1 = (bf16[32,256]{1,0:T(8,128)(2,1)S(1)}, bf16[32,256]{1,0:T(8,128)(2,1)}, u32[]{:S(2)}) copy-start(bf16[32,256]{1,0:T(8,128)(2,1)} %param.25) | copy-start | bytes 49156
  55.9 35.0 %copy-start.5 = (bf16[1024,256]{1,0:T(8,128)(2,1)S(1)}, bf16[1024,256]{1,0:T(8,128)(2,1)}, u32[]{:S(2)}) copy-start(bf16[1024,256]{1,0:T(8,128)(2,1)} %param.46) | copy-start | bytes 1572868
  73.2 34.9 %copy-start.16 = (f32[128]{0:T(128)S(1)}, f32[128]{0:T(128)}, u32[]{:S(2)}) copy-start(f32[128]{0:T(128)} %param.47) | copy-start | bytes 1540
  73.3 66.1 %copy-start.2 = (bf16[128,2048]{1,0:T(8,128)(2,1)S(1)}, bf16[128,2048]{1,0:T(8,128)(2,1)}, u32[]{:S(2)}) copy-start(bf16[128,2048]{1,0:T(8,128)(2,1)} %param.48) | copy-start | bytes 1572868
  84.9 17.4 %all-to-all-start.1 = ((bf16[16,2,1024]{2,1,0:T(2,128)(2,1)}), bf16[16,2,1024]{2,1,0:T(2,128)(2,1)S(1)}, u32[]{:S(2)}, u32[]{:S(2)}) async-start(bf16[16,2,1024]{2,1,0:T(2,128)(2,1)} %broadcast_in_dim.13), calls=%async_computation.1 | async-start | bytes 131072 | tf_op jit(solution)/shard_map/all_to_all | solution.py:42
  129.1 22.6 %all-to-all-start.4 = ((f32[32,1,256]{2,1,0:T(1,128)}), f32[32,1,256]{2,1,0:T(1,128)S(1)}, u32[]{:S(2)}, u32[]{:S(2)}) async-start(f32[32,1,256]{2,1,0:T(1,128)} %broadcast_in_dim.14), calls=%async_computation.4 | async-start | bytes 65536 | tf_op jit(solution)/shard_map/all_to_all | solution.py:42
  151.6 60.5 %all-to-all-start.3 = ((bf16[32,256,64]{1,2,0:T(8,128)(2,1)}), bf16[32,256,64]{1,2,0:T(8,128)(2,1)S(1)}, u32[]{:S(2)}, u32[]{:S(2)}) async-start(bf16[32,256,64]{1,2,0:T(8,128)(2,1)} %bitcast.41), calls=%async_computation.3 | async-start | bytes 2097152 | tf_op jit(solution)/shard_map/all_to_all | solution.py:74
